TPU v7x, 32 devices: a whole 2x2x4 slice. The times are simulated.
32 devices in a mesh: fs: 8 (over z, y), tp: 4 (over x, core).
Axes of the slice: x: 2, y: 2, z: 4, core: 2. Of those that a mesh axis runs over, the one named last changes fastest.
Arguments:
- tokens: bfloat16 [4096, 2048], P(('fs', 'tp')), may hold values from -6 to 6
- gate_proj: bfloat16 [2048, 512], P('fs', 'tp'), may hold values from -0.125 to 0.125
- signal_proj: bfloat16 [2048, 512], P('fs', 'tp'), may hold values from -1.5467961 to 1.5467961
- spatial: bfloat16 [4, 128, 128], replicated, may hold values from -0.5 to 0.5
- signal_gain: bfloat16 [512], P('tp'), may hold values from 0.099609375 to 1.8984375
- mixer_out: bfloat16 [512, 2048], P('tp', 'fs'), may hold values from -0.25 to 0.25
- mixer_gain: bfloat16 [2048], replicated, may hold values from 0.099609375 to 1.8984375
- ffn_gate: bfloat16 [2048, 5632], P('fs', 'tp'), may hold values from -0.125 to 0.125
- ffn_value: bfloat16 [2048, 5632], P('fs', 'tp'), may hold values from -0.125 to 0.125
- conv_taps: bfloat16 [3, 5632], P(None, 'tp'), may hold values from -3.5 to 3.5
- ffn_down: bfloat16 [5632, 2048], P('tp', 'fs'), may hold values from -0.078125 to 0.078125
- output_gain: bfloat16 [2048], replicated, may hold values from 0.099609375 to 1.8984375
Outputs:
- result: bfloat16 [4096, 2048], P(('fs', 'tp'))
All inputs are finite; a program needn't handle non-finite values.
Results may differ from a plain program's by a relative error of at most 0.01.
Values may be sent and summed in bfloat16 or wider, within the bound.
A program may use at most 64 MiB of HBM per device.

v0:
```python
import math
import jax
import jax.numpy as jnp
from jax import lax
from jax.sharding import PartitionSpec as P

MIX_WIDTH = 512
HEAD_SIZE = 128
BLOCK = 128
SEGMENT = 64
EPSILON = 1e-05
RESIDUAL_SCALE = math.sqrt(2.0)


def normalize(values):
    row_mean = jnp.mean(values, axis=-1, keepdims=True)
    centred = values - row_mean
    spread = jnp.mean(centred * centred, axis=-1, keepdims=True)
    return centred * lax.rsqrt(spread + EPSILON)


def causal_conv(gate_pre, conv_taps):
    taps = conv_taps.astype(jnp.float32)
    width = gate_pre.shape[1]
    shifted_one = jnp.concatenate([jnp.zeros((1, width), jnp.float32), gate_pre[:-1]], axis=0)
    shifted_two = jnp.concatenate([jnp.zeros((2, width), jnp.float32), gate_pre[:-2]], axis=0)
    return taps[0] * shifted_two + taps[1] * shifted_one + taps[2] * gate_pre


def shards(
    tokens,
    gate_proj,
    signal_proj,
    spatial,
    signal_gain,
    mixer_out,
    mixer_gain,
    ffn_gate,
    ffn_value,
    conv_taps,
    ffn_down,
    output_gain,
):
    residual = tokens.astype(jnp.float32)
    mix_input = normalize(residual).astype(jnp.bfloat16)
    segment_ids = jnp.arange(BLOCK) // SEGMENT
    allowed = segment_ids[None, :] <= segment_ids[:, None]
    masked = jnp.where(allowed[None], spatial, jnp.zeros_like(spatial))
    group_input = lax.all_gather(mix_input, "tp", axis=0, tiled=True)
    group_rows = group_input.shape[0]
    column_count = gate_proj.shape[1]
    pieces = (
        lax.all_gather(gate_proj, "fs", axis=0, tiled=True),
        lax.all_gather(signal_proj, "fs", axis=0, tiled=True),
    )
    left_part = group_input
    gate_sum = jnp.dot(left_part, pieces[0], preferred_element_type=jnp.float32)
    signal_sum = jnp.dot(left_part, pieces[1], preferred_element_type=jnp.float32)
    branch_gate = jax.nn.gelu(gate_sum)
    branch_signal = jax.nn.gelu(signal_sum)
    total_sum, square_sum = lax.psum(
        (jnp.sum(branch_signal, axis=1), jnp.sum(branch_signal * branch_signal, axis=1)), "tp"
    )
    row_mean = total_sum / MIX_WIDTH
    spread = square_sum / MIX_WIDTH - row_mean * row_mean
    spatial_input = (
        (branch_signal - row_mean[:, None])
        * lax.rsqrt(spread[:, None] + EPSILON)
        * signal_gain.astype(jnp.float32)
    ).astype(jnp.bfloat16)
    head_index = lax.axis_index("tp") * column_count // HEAD_SIZE
    own_weights = lax.dynamic_index_in_dim(masked, head_index, 0, keepdims=False)
    blocks = spatial_input.reshape(group_rows // BLOCK, BLOCK, column_count)
    mixed_rows = jnp.einsum(
        "ij,njc->nic", own_weights, blocks, preferred_element_type=jnp.float32
    ).reshape(group_rows, column_count)
    gated_rows = (branch_gate * mixed_rows).astype(jnp.bfloat16)
    out_columns = lax.all_gather(mixer_out, "fs", axis=1, tiled=True)
    selected = gated_rows
    mix_out = lax.psum_scatter(
        jnp.dot(selected, out_columns, preferred_element_type=jnp.float32).astype(jnp.bfloat16),
        "tp",
        scatter_dimension=0,
        tiled=True,
    ).astype(jnp.float32)
    middle = (
        normalize(RESIDUAL_SCALE * residual + mix_out) * mixer_gain.astype(jnp.float32)
    ).astype(jnp.bfloat16)
    middle_wide = middle.astype(jnp.float32)
    ffn_input = normalize(middle_wide).astype(jnp.bfloat16)
    group_ffn = lax.all_gather(ffn_input, "tp", axis=0, tiled=True)
    pieces = (
        lax.all_gather(ffn_gate, "fs", axis=0, tiled=True),
        lax.all_gather(ffn_value, "fs", axis=0, tiled=True),
    )
    left_part = group_ffn
    gate_pre = jnp.dot(left_part, pieces[0], preferred_element_type=jnp.float32)
    value_pre = jnp.dot(left_part, pieces[1], preferred_element_type=jnp.float32)
    whole_down = lax.all_gather(ffn_down, "fs", axis=1, tiled=True)
    hidden = (jax.nn.silu(causal_conv(gate_pre, conv_taps)) * value_pre).astype(jnp.bfloat16)
    selected = hidden
    ffn_out = lax.psum_scatter(
        jnp.dot(selected, whole_down, preferred_element_type=jnp.float32).astype(jnp.bfloat16),
        "tp",
        scatter_dimension=0,
        tiled=True,
    ).astype(jnp.float32)
    return (
        normalize(RESIDUAL_SCALE * middle_wide + ffn_out) * output_gain.astype(jnp.float32)
    ).astype(jnp.bfloat16)


def solution(mesh):
    in_specs = (
        P(("fs", "tp"), None),
        P("fs", "tp"),
        P("fs", "tp"),
        P(),
        P("tp"),
        P("tp", "fs"),
        P(),
        P("fs", "tp"),
        P("fs", "tp"),
        P(None, "tp"),
        P("tp", "fs"),
        P(),
    )
    out_specs = P(("fs", "tp"), None)
    return jax.shard_map(shards, mesh=mesh, in_specs=in_specs, out_specs=out_specs, check_vma=False)
```

profile of v0, /device:TPU:0, one launch (start us, length us, event | category | flops | bytes accessed | tf_op | source)
XLA Modules:
  0.0 485.2 jit_solution(16382907867453121920)
XLA Ops:
  7.4 1.2 convert_reduce_fusion.1
  8.6 1.3 fusion.7
  9.9 2.2 fusion.8
  12.1 0.0 all-gather.6.cloned.1.call-update
  12.1 0.0 reduce-scatter.3.cloned.1.call-start
  12.2 0.7 convert_element_type.53
  12.9 0.1 broadcast_compare_fusion
  13.0 33.3 %all_gather.26 = bf16[2048,128]{1,0:T(8,128)(2,1)S(1)} all-gather(bf16[256,128]{1,0:T(8,128)(2,1)} %param.14), channel_id=1, replica_groups=mesh['fs'=8,'tp'=4] {'fs'}, dimensions={0}, use_global_device_ids=true | all-gather | bytes 589824 | tf_op jit(solution)/shard_map/all_gather | solution.py:54
  46.3 31.5 %all_gather.25 = bf16[2048,128]{1,0:T(8,128)(2,1)S(1)} all-gather(bf16[256,128]{1,0:T(8,128)(2,1)S(1)} %copy-done.1), channel_id=1, replica_groups=mesh['fs'=8,'tp'=4] {'fs'}, dimensions={0}, use_global_device_ids=true | all-gather | bytes 589824 | tf_op jit(solution)/shard_map/all_gather | solution.py:53
  77.8 0.0 copy-done.2
  77.8 31.2 %all_gather.27 = bf16[128,2048]{1,0:T(8,128)(2,1)S(1)} all-gather(bf16[128,256]{1,0:T(8,128)(2,1)S(1)} %copy-done.2), channel_id=1, replica_groups=mesh['fs'=8,'tp'=4] {'fs'}, dimensions={1}, use_global_device_ids=true | all-gather | bytes 589824 | tf_op jit(solution)/shard_map/all_gather | solution.py:78
  109.0 2.4 fusion.38
  111.4 5.7 %all-reduce.2 = (f32[512]{0:T(512)S(1)}, f32[512]{0:T(512)S(1)}) all-reduce(f32[512]{0:T(512)S(1)} %get-tuple-element.6, f32[512]{0:T(512)S(1)} %get-tuple-element.5), channel_id=1, replica_groups=mesh['fs'=8,'tp'=4] {'tp'}, use_global_device_ids=true, to_apply=%region_5.6 | all-reduce | flops 1024 | bytes 8192 | tf_op jit(solution)/shard_map/psum | solution.py:61
  117.1 0.2 multiply_convert_fusion.2
  117.3 0.9 fusion.30
  118.2 2.3 fusion.21
  120.6 0.0 copy-start.4
  120.6 0.0 copy-start
  120.6 2.0 convolution_convert_fusion
  122.6 0.0 reduce-scatter.3.cloned.1.call-update
  122.6 0.0 all-gather.10.cloned.1.call-start
  122.7 0.5 all-gather.10.cloned.1.call-update
  123.2 0.0 all-gather.8.cloned.1.call-start
  123.3 31.8 %reduce-scatter.3.cloned.1.call-done = bf16[128,2048]{1,0:T(8,128)(2,1)} async-done(((bf16[512,2048]{1,0:T(8,128)(2,1)}), bf16[128,2048]{1,0:T(8,128)(2,1)}) %reduce-scatter.3.cloned.1.call-update) | async-done | bytes 524304 | tf_op jit(solution)/shard_map/reduce_scatter | solution.py:80
  155.1 1.3 fusion.12
  156.4 1.4 multiply_reduce_fusion.1
  157.8 1.4 convert_reduce_fusion
  159.3 0.3 fusion.5
  159.6 1.1 fusion.6
  160.7 0.0 all-gather.8.cloned.1.call-update
  160.7 0.0 all-gather.12.cloned.1.call-start
  160.7 0.5 all-gather.12.cloned.1.call-update
  161.3 0.0 all-gather.14.cloned.1.call-start
  161.3 0.7 all-gather.14.cloned.1.call-update
  162.0 0.2 reduce-scatter.5.cloned.1.call-start
  162.3 0.1 slice_reduce_fusion.2
  162.3 56.3 %all-gather.10.cloned.1.call-done = bf16[2048,1408]{1,0:T(8,128)(2,1)} async-done(((bf16[256,1408]{1,0:T(8,128)(2,1)}), bf16[2048,1408]{1,0:T(8,128)(2,1)}) %all-gather.10.cloned.1.call-update) | async-done | bytes 5767184 | tf_op jit(solution)/shard_map/all_gather | solution.py:93
  218.6 22.0 %all-gather.8.cloned.1.call-done = bf16[512,2048]{1,0:T(8,128)(2,1)} async-done(((bf16[128,2048]{1,0:T(8,128)(2,1)}), bf16[512,2048]{1,0:T(8,128)(2,1)}) %all-gather.8.cloned.1.call-update) | async-done | bytes 2097168 | tf_op jit(solution)/shard_map/all_gather | solution.py:91
  240.6 8.4 %fusion.39 = f32[512,1408]{1,0:T(8,128)} fusion(bf16[512,2048]{1,0:T(8,128)(2,1)} %all-gather.8.cloned.1.call-done, bf16[2048,1408]{1,0:T(8,128)(2,1)} %all-gather.10.cloned.1.call-done), kind=kOutput, calls=%fused_computation.74 | convolution fusion | flops 2952790016 | bytes 10747904 | tf_op jit(solution)/shard_map/dot_general | solution.py:97
  249.0 85.8 %all-gather.12.cloned.1.call-done = bf16[2048,1408]{1,0:T(8,128)(2,1)} async-done(((bf16[256,1408]{1,0:T(8,128)(2,1)}), bf16[2048,1408]{1,0:T(8,128)(2,1)}) %all-gather.12.cloned.1.call-update) | async-done | bytes 5767184 | tf_op jit(solution)/shard_map/all_gather | solution.py:94
  334.8 93.1 %all-gather.14.cloned.1.call-done = bf16[1408,2048]{1,0:T(8,128)(2,1)} async-done(((bf16[1408,256]{1,0:T(8,128)(2,1)}), bf16[1408,2048]{1,0:T(8,128)(2,1)}) %all-gather.14.cloned.1.call-update) | async-done | bytes 5767184 | tf_op jit(solution)/shard_map/all_gather | solution.py:99
  428.0 15.5 %convolution_convert_fusion.1 = bf16[512,2048]{1,0:T(8,128)(2,1)} fusion(bf16[1408,2048]{1,0:T(8,128)(2,1)} %all-gather.14.cloned.1.call-done, bf16[512,2048]{1,0:T(8,128)(2,1)S(1)} %copy-done.6, bf16[2048,1408]{1,0:T(8,128)(2,1)} %all-gather.12.cloned.1.call-done, f32[512,1408]{1,0:T(8,128)} %fusion.39, f32[511,1408]{1,0:T(8,128)} %bitcast.24, ...), kind=kOutput, calls=%fused_computation.3 | convolution fusion | flops 5914558464 | bytes 24379392 | tf_op jit(solution)/shard_map/dot_general | solution.py:103
  443.5 0.0 reduce-scatter.5.cloned.1.call-update
  443.5 0.0 copy-done.5
  443.6 29.5 %reduce-scatter.5.cloned.1.call-done = bf16[128,2048]{1,0:T(8,128)(2,1)} async-done(((bf16[512,2048]{1,0:T(8,128)(2,1)}), bf16[128,2048]{1,0:T(8,128)(2,1)}) %reduce-scatter.5.cloned.1.call-update) | async-done | bytes 524304 | tf_op jit(solution)/shard_map/reduce_scatter | solution.py:102
  473.0 1.3 fusion.11
  474.3 1.4 multiply_reduce_fusion
  475.7 2.1 multiply_convert_fusion
  (25 shorter events, 0.1 us)
Async XLA Ops:
  7.4 38.9 %copy-start.1 = (bf16[256,128]{1,0:T(8,128)(2,1)S(1)}, bf16[256,128]{1,0:T(8,128)(2,1)}, u32[]{:S(2)}) copy-start(bf16[256,128]{1,0:T(8,128)(2,1)} %param.13) | copy-start | bytes 196612
  7.4 70.4 %copy-start.2 = (bf16[128,256]{1,0:T(8,128)(2,1)S(1)}, bf16[128,256]{1,0:T(8,128)(2,1)}, u32[]{:S(2)}) copy-start(bf16[128,256]{1,0:T(8,128)(2,1)} %param.17) | copy-start | bytes 196612
  7.4 101.6 %all-gather.6.cloned.1.call-start = ((), (), s32[]{:S(2)}) async-start(), calls=%async_computation.2 | async-start | bytes 2621440 | tf_op jit(solution)/shard_map/all_gather | solution.py:49
  12.1 143.0 %reduce-scatter.3.cloned.1.call-start = ((), (), s32[]{:S(2)}) async-start(), calls=%async_computation.3 | async-start | bytes 2621440 | tf_op jit(solution)/shard_map/reduce_scatter | solution.py:80
  120.6 2.7 copy-start.4
  120.6 34.5 %copy-start = (bf16[128,2048]{1,0:T(8,128)(2,1)S(1)}, bf16[128,2048]{1,0:T(8,128)(2,1)}, u32[]{:S(2)}) copy-start(bf16[128,2048]{1,0:T(8,128)(2,1)} %param.12) | copy-start | bytes 1572868
  122.6 96.0 %all-gather.10.cloned.1.call-start = ((), (), s32[]{:S(2)}) async-start(), calls=%async_computation.5 | async-start | bytes 6488064 | tf_op jit(solution)/shard_map/all_gather | solution.py:93
  123.2 117.4 %all-gather.8.cloned.1.call-start = ((), (), s32[]{:S(2)}) async-start(), calls=%async_computation.4 | async-start | bytes 2621440 | tf_op jit(solution)/shard_map/all_gather | solution.py:91
  156.4 5.8 %copy-start.3 = (bf16[3,1408]{1,0:T(4,128)(2,1)S(1)}, bf16[3,1408]{1,0:T(4,128)(2,1)}, u32[]{:S(2)}) copy-start(bf16[3,1408]{1,0:T(4,128)(2,1)} %param.21) | copy-start | bytes 25348
  160.7 174.2 %all-gather.12.cloned.1.call-start = ((), (), s32[]{:S(2)}) async-start(), calls=%async_computation.6 | async-start | bytes 6488064 | tf_op jit(solution)/shard_map/all_gather | solution.py:94
  161.3 266.7 %all-gather.14.cloned.1.call-start = ((), (), s32[]{:S(2)}) async-start(), calls=%async_computation.7 | async-start | bytes 6488064 | tf_op jit(solution)/shard_map/all_gather | solution.py:99
  162.0 311.0 %reduce-scatter.5.cloned.1.call-start = ((), (), s32[]{:S(2)}) async-start(), calls=%async_computation.8 | async-start | bytes 2621440 | tf_op jit(solution)/shard_map/reduce_scatter | solution.py:102
  240.6 187.3 %copy-start.6 = (bf16[512,2048]{1,0:T(8,128)(2,1)S(1)}, bf16[512,2048]{1,0:T(8,128)(2,1)}, u32[]{:S(2)}) copy-start(bf16[512,2048]{1,0:T(8,128)(2,1)} %all-gather.8.cloned.1.call-done) | copy-start | bytes 6291460
  428.0 15.6 %copy-start.5 = (bf16[2048]{0:T(1024)(128)(2,1)S(1)}, bf16[2048]{0:T(1024)(128)(2,1)}, u32[]{:S(2)}) copy-start(bf16[2048]{0:T(1024)(128)(2,1)} %param.23) | copy-start | bytes 12292
Sparse Core Ops, SparseCore 0:
  12.2 25.2 all-gather.5
  122.8 32.3 reduce-scatter.2
  443.6 29.3 reduce-scatter.4
Sparse Core Ops, SparseCore 1:
  125.3 93.2 all-gather.9
  220.0 20.5 all-gather.7
  242.7 92.1 all-gather.11
  336.9 91.0 all-gather.13
where the time goes:
time: 486 us; the launch traced here: 485 us
  waiting for transfers between devices  320 us (66%)
  blocking collectives  102 us (21%)
  matrix products  31.6 us (7%)
  other arithmetic  16 us (3%)
  between operations  15 us (3%)
    all_gather x1, waiting for transfers between devices, shards(): whole_down = lax.all_gather(ffn_down, 'fs', axis=1, tiled=True)  93.1 us
    all_gather x1, waiting for transfers between devices, shards(): lax.all_gather(ffn_value, 'fs', axis=0, tiled=True)  85.8 us
    all_gather x1, waiting for transfers between devices, shards(): lax.all_gather(ffn_gate, 'fs', axis=0, tiled=True)  56.3 us
    all_gather x1, blocking collectives, shards(): lax.all_gather(signal_proj, 'fs', axis=0, tiled=True)  33.3 us
    reduce_scatter x1, waiting for transfers between devices, shards(): lax.psum_scatter(jnp.dot(selected, out_columns, preferred_element_type=jn...  31.8 us
    all_gather x1, blocking collectives, shards(): lax.all_gather(gate_proj, 'fs', axis=0, tiled=True)  31.5 us
    all_gather x1, blocking collectives, shards(): out_columns = lax.all_gather(mixer_out, 'fs', axis=1, tiled=True)  31.2 us
    reduce_scatter x1, waiting for transfers between devices, shards(): lax.psum_scatter(jnp.dot(selected, whole_down, preferred_element_type=jnp...  29.5 us
  transfers between devices with their start and end apart: 7, of which 6 were waited for; matrix products, arithmetic and copies ran while one was open for 3% of the time, Pallas kernels for 0%

commit v1 on v0

--- a/solution.py
+++ b/solution.py
@@ -96,7 +96,12 @@
     left_part = group_ffn
     gate_pre = jnp.dot(left_part, pieces[0], preferred_element_type=jnp.float32)
     value_pre = jnp.dot(left_part, pieces[1], preferred_element_type=jnp.float32)
-    whole_down = lax.all_gather(ffn_down, "fs", axis=1, tiled=True)
+    ring = [ffn_down]
+    for hop in range(7):
+        ring.append(lax.ppermute(ring[-1], "fs", [(dev, (dev + 1) % 8) for dev in range(8)]))
+    whole_down = jnp.roll(
+        jnp.concatenate(ring[::-1], axis=1), (lax.axis_index("fs") + 1) * ring[0].shape[1], axis=1
+    )
     hidden = (jax.nn.silu(causal_conv(gate_pre, conv_taps)) * value_pre).astype(jnp.bfloat16)
     selected = hidden
     ffn_out = lax.psum_scatter(

time: 486 us -> 458 us (0.942)
  waiting for transfers between devices: 320 us -> 267 us
  local copies, waits for them, and re-layouts: 0.08 us -> 23 us
    ppermute x0 -> x7, waiting for transfers between devices: none -> 202 us  [shards(): lax.ppermute(ring[-1], 'fs', [(dev, (dev + 1) % 8) for dev in range(8)])]
    all_gather x1 -> x0, waiting for transfers between devices: 93.1 us -> none  [shards(): whole_down = lax.all_gather(ffn_down, 'fs', axis=1, tiled=True)]
    all_gather x1, waiting for transfers between devices: 85.8 us -> 1.99 us  [shards(): lax.all_gather(ffn_value, 'fs', axis=0, tiled=True)]
    all_gather x1, waiting for transfers between devices: 56.3 us -> 0.01 us  [shards(): lax.all_gather(ffn_gate, 'fs', axis=0, tiled=True)]
    all_gather x1, waiting for transfers between devices: 22 us -> 0.01 us  [shards(): group_ffn = lax.all_gather(ffn_input, 'tp', axis=0, tiled=True)]
    unnamed x14 -> x35, local copies, waits for them, and re-layouts: 0.03 us -> 22 us
  transfers between devices with their start and end apart: 7 -> 13, of which waited for: 6 -> 10; matrix products, arithmetic and copies ran while one was open for 3% -> 8% of each run, Pallas kernels for 0% -> 0%
where the time goes in v1:
time: 458 us; the launch traced here: 457 us
  waiting for transfers between devices  267 us (58%)
  blocking collectives  102 us (22%)
  matrix products  32 us (7%)
  local copies, waits for them, and re-layouts  23 us (5%)
  other arithmetic  16 us (3%)
  between operations  14.9 us (3%)
    ppermute x7, waiting for transfers between devices, shards(): lax.ppermute(ring[-1], 'fs', [(dev, (dev + 1) % 8) for dev in range(8)])  202 us
    all_gather x1, blocking collectives, shards(): lax.all_gather(signal_proj, 'fs', axis=0, tiled=True)  33.3 us
    reduce_scatter x1, waiting for transfers between devices, shards(): lax.psum_scatter(jnp.dot(selected, out_columns, preferred_element_type=jn...  32 us
    all_gather x1, blocking collectives, shards(): lax.all_gather(gate_proj, 'fs', axis=0, tiled=True)  31.5 us
    all_gather x1, blocking collectives, shards(): out_columns = lax.all_gather(mixer_out, 'fs', axis=1, tiled=True)  31.5 us
    reduce_scatter x1, waiting for transfers between devices, shards(): lax.psum_scatter(jnp.dot(selected, whole_down, preferred_element_type=jnp...  30.2 us
    unnamed x35, local copies, waits for them, and re-layouts  22 us
    dot_general x1, matrix products, shards(): jnp.dot(selected, whole_down, preferred_element_type=jnp.float32)  15.7 us
  transfers between devices with their start and end apart: 13, of which 10 were waited for; matrix products, arithmetic and copies ran while one was open for 8% of the time, Pallas kernels for 0%

profile of v1, /device:TPU:0, one launch (start us, length us, event | category | flops | bytes accessed | tf_op | source)
XLA Modules:
  0.0 457.4 jit_solution(10864396581177287229)
XLA Ops:
  7.4 1.2 convert_reduce_fusion.1
  8.6 1.3 fusion.12
  9.9 2.2 fusion.13
  12.9 33.3 %all_gather.23 = bf16[2048,128]{1,0:T(8,128)(2,1)S(1)} all-gather(bf16[256,128]{1,0:T(8,128)(2,1)} %param.14), channel_id=1, replica_groups=mesh['fs'=8,'tp'=4] {'fs'}, dimensions={0}, use_global_device_ids=true | all-gather | bytes 589824 | tf_op jit(solution)/shard_map/all_gather | solution.py:54
  46.2 31.5 %all_gather.22 = bf16[2048,128]{1,0:T(8,128)(2,1)S(1)} all-gather(bf16[256,128]{1,0:T(8,128)(2,1)} %param.13), channel_id=1, replica_groups=mesh['fs'=8,'tp'=4] {'fs'}, dimensions={0}, use_global_device_ids=true | all-gather | bytes 589824 | tf_op jit(solution)/shard_map/all_gather | solution.py:53
  77.7 31.5 %all_gather.24 = bf16[128,2048]{1,0:T(8,128)(2,1)S(1)} all-gather(bf16[128,256]{1,0:T(8,128)(2,1)} %param.17), channel_id=1, replica_groups=mesh['fs'=8,'tp'=4] {'fs'}, dimensions={1}, use_global_device_ids=true | all-gather | bytes 589824 | tf_op jit(solution)/shard_map/all_gather | solution.py:78
  109.3 2.5 fusion.44
  111.8 5.7 %all-reduce.2 = (f32[512]{0:T(512)S(1)}, f32[512]{0:T(512)S(1)}) all-reduce(f32[512]{0:T(512)S(1)} %get-tuple-element.6, f32[512]{0:T(512)S(1)} %get-tuple-element.5), channel_id=1, replica_groups=mesh['fs'=8,'tp'=4] {'tp'}, use_global_device_ids=true, to_apply=%region_5.6 | all-reduce | flops 1024 | bytes 8192 | tf_op jit(solution)/shard_map/psum | solution.py:61
  117.7 0.9 fusion.35
  118.6 2.3 fusion.26
  120.9 2.0 convolution_convert_fusion
  123.7 32.0 %reduce-scatter.3.cloned.1.call-done = bf16[128,2048]{1,0:T(8,128)(2,1)} async-done(((bf16[512,2048]{1,0:T(8,128)(2,1)}), bf16[128,2048]{1,0:T(8,128)(2,1)}) %reduce-scatter.3.cloned.1.call-update) | async-done | bytes 524304 | tf_op jit(solution)/shard_map/reduce_scatter | solution.py:80
  155.7 1.3 fusion.17
  157.0 1.4 multiply_reduce_fusion.1
  158.4 1.4 convert_reduce_fusion
  160.1 1.1 fusion.11
  161.9 1.5 collective-permute-start
  163.4 30.7 %collective-permute-done = bf16[1408,256]{1,0:T(8,128)(2,1)S(1)} collective-permute-done((bf16[1408,256]{1,0:T(8,128)(2,1)S(1)}, bf16[1408,256]{1,0:T(8,128)(2,1)S(1)}, u32[]{:S(2)}, u32[]{:S(2)}) %collective-permute-start) | collective-permute-done | bytes 720928 | tf_op jit(solution)/shard_map/ppermute | solution.py:101
  194.3 35.4 %collective-permute-done.1 = bf16[1408,256]{1,0:T(8,128)(2,1)S(1)} collective-permute-done((bf16[1408,256]{1,0:T(8,128)(2,1)S(1)}, bf16[1408,256]{1,0:T(8,128)(2,1)S(1)}, u32[]{:S(2)}, u32[]{:S(2)}) %collective-permute-start.1) | collective-permute-done | bytes 720928 | tf_op jit(solution)/shard_map/ppermute | solution.py:101
  229.7 30.0 %collective-permute-done.2 = bf16[1408,256]{1,0:T(8,128)(2,1)S(1)} collective-permute-done((bf16[1408,256]{1,0:T(8,128)(2,1)S(1)}, bf16[1408,256]{1,0:T(8,128)(2,1)S(1)}, u32[]{:S(2)}, u32[]{:S(2)}) %collective-permute-start.2) | collective-permute-done | bytes 720928 | tf_op jit(solution)/shard_map/ppermute | solution.py:101
  259.7 0.9 copy-done.2
  260.6 19.1 %collective-permute-done.3 = bf16[1408,256]{1,0:T(8,128)(2,1)S(1)} collective-permute-done((bf16[1408,256]{1,0:T(8,128)(2,1)S(1)}, bf16[1408,256]{1,0:T(8,128)(2,1)S(1)}, u32[]{:S(2)}, u32[]{:S(2)}) %collective-permute-start.3) | collective-permute-done | bytes 720928 | tf_op jit(solution)/shard_map/ppermute | solution.py:101
  279.6 23.8 %collective-permute-done.4 = bf16[1408,256]{1,0:T(8,128)(2,1)S(1)} collective-permute-done((bf16[1408,256]{1,0:T(8,128)(2,1)S(1)}, bf16[1408,256]{1,0:T(8,128)(2,1)S(1)}, u32[]{:S(2)}, u32[]{:S(2)}) %collective-permute-start.4) | collective-permute-done | bytes 720928 | tf_op jit(solution)/shard_map/ppermute | solution.py:101
  304.3 33.5 %collective-permute-done.5 = bf16[1408,256]{1,0:T(8,128)(2,1)} collective-permute-done((bf16[1408,256]{1,0:T(8,128)(2,1)S(1)}, bf16[1408,256]{1,0:T(8,128)(2,1)}, u32[]{:S(2)}, u32[]{:S(2)}) %collective-permute-start.5) | collective-permute-done | bytes 720928 | tf_op jit(solution)/shard_map/ppermute | solution.py:101
  337.9 29.7 %collective-permute-done.6 = bf16[1408,256]{1,0:T(8,128)(2,1)} collective-permute-done((bf16[1408,256]{1,0:T(8,128)(2,1)}, bf16[1408,256]{1,0:T(8,128)(2,1)}, u32[]{:S(2)}, u32[]{:S(2)}) %collective-permute-start.6) | collective-permute-done | bytes 720928 | tf_op jit(solution)/shard_map/ppermute | solution.py:101
  367.6 2.1 constant_dynamic-update-slice_fusion.15
  369.8 2.1 constant_dynamic-update-slice_fusion.14
  371.8 2.1 constant_dynamic-update-slice_fusion.13
  374.0 1.0 constant_dynamic-update-slice_fusion.12
  375.0 0.9 constant_dynamic-update-slice_fusion.11
  376.0 1.0 constant_dynamic-update-slice_fusion.10
  376.9 1.0 constant_dynamic-update-slice_fusion.9
  377.9 1.0 constant_dynamic-update-slice_fusion.8
  378.8 2.1 constant_dynamic-update-slice_fusion.7
  380.9 2.1 constant_dynamic-update-slice_fusion.6
  383.0 0.9 constant_dynamic-update-slice_fusion.5
  384.0 0.9 constant_dynamic-update-slice_fusion.4
  384.9 1.0 constant_dynamic-update-slice_fusion.3
  385.9 1.0 constant_dynamic-update-slice_fusion.2
  386.9 1.0 constant_dynamic-update-slice_fusion.1
  387.9 1.0 constant_dynamic-update-slice_fusion
  388.8 8.5 %fusion.45 = f32[512,1408]{1,0:T(8,128)} fusion(bf16[512,2048]{1,0:T(8,128)(2,1)} %all-gather.7.cloned.1.call-done, bf16[2048,1408]{1,0:T(8,128)(2,1)} %all-gather.9.cloned.1.call-done), kind=kOutput, calls=%fused_computation.93 | convolution fusion | flops 2952790016 | bytes 10747904 | tf_op jit(solution)/shard_map/dot_general | solution.py:97
  397.3 2.0 all-gather.11.cloned.1.call-done
  399.3 15.7 %fusion.3 = bf16[512,2048]{1,0:T(8,128)(2,1)} fusion(bf16[1408,4096]{1,0:T(8,128)(2,1)} %constant_dynamic-update-slice_fusion, s32[]{:T(128)S(6)} %select_n.43, bf16[512,2048]{1,0:T(8,128)(2,1)S(1)} %copy-done.9, bf16[2048,1408]{1,0:T(8,128)(2,1)} %all-gather.11.cloned.1.call-done, f32[512,1408]{1,0:T(8,128)} %fusion.45, f32[511,1408]{1,0:T(8,128)} %bitcast.23, ...), kind=kOutput, calls=%fused_computation.5 | convolution fusion | flops 5914558464 | bytes 24396292 | tf_op jit(solution)/shard_map/dot_general | solution.py:108
  415.1 30.2 %reduce-scatter.5.cloned.1.call-done = bf16[128,2048]{1,0:T(8,128)(2,1)} async-done(((bf16[512,2048]{1,0:T(8,128)(2,1)}), bf16[128,2048]{1,0:T(8,128)(2,1)}) %reduce-scatter.5.cloned.1.call-update) | async-done | bytes 524304 | tf_op jit(solution)/shard_map/reduce_scatter | solution.py:107
  445.3 1.3 fusion.16
  446.6 1.4 multiply_reduce_fusion
  448.0 2.1 multiply_convert_fusion
  (58 shorter events, 3.9 us)
Async XLA Ops:
  7.4 101.9 %all-gather.5.cloned.1.call-start = ((), (), s32[]{:S(2)}) async-start(), calls=%async_computation.2 | async-start | bytes 2621440 | tf_op jit(solution)/shard_map/all_gather | solution.py:49
  12.1 143.6 %reduce-scatter.3.cloned.1.call-start = ((), (), s32[]{:S(2)}) async-start(), calls=%async_computation.3 | async-start | bytes 2621440 | tf_op jit(solution)/shard_map/reduce_scatter | solution.py:80
  109.3 14.4 %copy-start.7 = (bf16[2048]{0:T(1024)(128)(2,1)S(1)}, bf16[2048]{0:T(1024)(128)(2,1)}, u32[]{:S(2)}) copy-start(bf16[2048]{0:T(1024)(128)(2,1)} %param.18) | copy-start | bytes 12292
  109.3 46.4 %copy-start = (bf16[128,2048]{1,0:T(8,128)(2,1)S(1)}, bf16[128,2048]{1,0:T(8,128)(2,1)}, u32[]{:S(2)}) copy-start(bf16[128,2048]{1,0:T(8,128)(2,1)} %param.12) | copy-start | bytes 1572868
  120.9 41.0 %copy-start.1 = (bf16[1408,256]{1,0:T(8,128)(2,1)S(1)}, bf16[1408,256]{1,0:T(8,128)(2,1)}, u32[]{:S(2)}) copy-start(bf16[1408,256]{1,0:T(8,128)(2,1)} %param.22) | copy-start | bytes 2162692
  120.9 216.9 %copy-start.6 = (bf16[3,1408]{1,0:T(4,128)(2,1)S(1)}, bf16[3,1408]{1,0:T(4,128)(2,1)}, u32[]{:S(2)}) copy-start(bf16[3,1408]{1,0:T(4,128)(2,1)} %param.21) | copy-start | bytes 25348
  123.0 265.8 %all-gather.9.cloned.1.call-start = ((), (), s32[]{:S(2)}) async-start(), calls=%async_computation.5 | async-start | bytes 6488064 | tf_op jit(solution)/shard_map/all_gather | solution.py:93
  123.6 265.3 %all-gather.7.cloned.1.call-start = ((), (), s32[]{:S(2)}) async-start(), calls=%async_computation.4 | async-start | bytes 2621440 | tf_op jit(solution)/shard_map/all_gather | solution.py:91
  161.2 238.1 %all-gather.11.cloned.1.call-start = ((), (), s32[]{:S(2)}) async-start(), calls=%async_computation.6 | async-start | bytes 6488064 | tf_op jit(solution)/shard_map/all_gather | solution.py:94
  161.8 283.5 %reduce-scatter.5.cloned.1.call-start = ((), (), s32[]{:S(2)}) async-start(), calls=%async_computation.7 | async-start | bytes 2621440 | tf_op jit(solution)/shard_map/reduce_scatter | solution.py:107
  161.9 32.2 %collective-permute-start = (bf16[1408,256]{1,0:T(8,128)(2,1)S(1)}, bf16[1408,256]{1,0:T(8,128)(2,1)S(1)}, u32[]{:S(2)}, u32[]{:S(2)}) collective-permute-start(bf16[1408,256]{1,0:T(8,128)(2,1)S(1)} %copy-done.1), channel_id=1, source_target_pairs={{0,4},{4,8},{8,12},{12,16},{16,20},{20,24},{24,28},{28,0},{1,5},{5... | collective-permute-start | bytes 2162696 | tf_op jit(solution)/shard_map/ppermute | solution.py:101
  194.1 35.6 %collective-permute-start.1 = (bf16[1408,256]{1,0:T(8,128)(2,1)S(1)}, bf16[1408,256]{1,0:T(8,128)(2,1)S(1)}, u32[]{:S(2)}, u32[]{:S(2)}) collective-permute-start(bf16[1408,256]{1,0:T(8,128)(2,1)S(1)} %collective-permute-done), channel_id=1, source_target_pairs={{0,4},{4,8},{8,12},{12,16},{16,20},{20,24},{24,28},{28,0},{1,5},{5... | collective-permute-start | bytes 2162696 | tf_op jit(solution)/shard_map/ppermute | solution.py:101
  229.7 30.0 %collective-permute-start.2 = (bf16[1408,256]{1,0:T(8,128)(2,1)S(1)}, bf16[1408,256]{1,0:T(8,128)(2,1)S(1)}, u32[]{:S(2)}, u32[]{:S(2)}) collective-permute-start(bf16[1408,256]{1,0:T(8,128)(2,1)S(1)} %collective-permute-done.1), channel_id=1, source_target_pairs={{0,4},{4,8},{8,12},{12,16},{16,20},{20,24},{24,28},{28,0},{1,5},{5... | collective-permute-start | bytes 2162696 | tf_op jit(solution)/shard_map/ppermute | solution.py:101
  259.7 0.9 copy-start.2
  260.6 19.1 %collective-permute-start.3 = (bf16[1408,256]{1,0:T(8,128)(2,1)S(1)}, bf16[1408,256]{1,0:T(8,128)(2,1)S(1)}, u32[]{:S(2)}, u32[]{:S(2)}) collective-permute-start(bf16[1408,256]{1,0:T(8,128)(2,1)S(1)} %collective-permute-done.2), channel_id=1, source_target_pairs={{0,4},{4,8},{8,12},{12,16},{16,20},{20,24},{24,28},{28,0},{1,5},{5... | collective-permute-start | bytes 2162696 | tf_op jit(solution)/shard_map/ppermute | solution.py:101
  279.6 23.8 %collective-permute-start.4 = (bf16[1408,256]{1,0:T(8,128)(2,1)S(1)}, bf16[1408,256]{1,0:T(8,128)(2,1)S(1)}, u32[]{:S(2)}, u32[]{:S(2)}) collective-permute-start(bf16[1408,256]{1,0:T(8,128)(2,1)S(1)} %collective-permute-done.3), channel_id=1, source_target_pairs={{0,4},{4,8},{8,12},{12,16},{16,20},{20,24},{24,28},{28,0},{1,5},{5... | collective-permute-start | bytes 2162696 | tf_op jit(solution)/shard_map/ppermute | solution.py:101
  303.4 0.9 copy-start.4
  304.3 33.5 %collective-permute-start.5 = (bf16[1408,256]{1,0:T(8,128)(2,1)S(1)}, bf16[1408,256]{1,0:T(8,128)(2,1)}, u32[]{:S(2)}, u32[]{:S(2)}) collective-permute-start(bf16[1408,256]{1,0:T(8,128)(2,1)S(1)} %collective-permute-done.4), channel_id=1, source_target_pairs={{0,4},{4,8},{8,12},{12,16},{16,20},{20,24},{24,28},{28,0},{1,5},{5... | collective-permute-start | bytes 2162696 | tf_op jit(solution)/shard_map/ppermute | solution.py:101
  337.8 29.8 %collective-permute-start.6 = (bf16[1408,256]{1,0:T(8,128)(2,1)}, bf16[1408,256]{1,0:T(8,128)(2,1)}, u32[]{:S(2)}, u32[]{:S(2)}) collective-permute-start(bf16[1408,256]{1,0:T(8,128)(2,1)} %collective-permute-done.5), channel_id=1, source_target_pairs={{0,4},{4,8},{8,12},{12,16},{16,20},{20,24},{24,28},{28,0},{1,5},{5... | collective-permute-start | bytes 2162696 | tf_op jit(solution)/shard_map/ppermute | solution.py:101
  337.8 37.2 %copy-start.3 = (bf16[1408,256]{1,0:T(8,128)(2,1)S(1)}, bf16[1408,256]{1,0:T(8,128)(2,1)}, u32[]{:S(2)}) copy-start(bf16[1408,256]{1,0:T(8,128)(2,1)} %copy-done.2) | copy-start | bytes 2162692
  371.8 11.2 %copy-start.5 = (bf16[1408,256]{1,0:T(8,128)(2,1)S(1)}, bf16[1408,256]{1,0:T(8,128)(2,1)}, u32[]{:S(2)}) copy-start(bf16[1408,256]{1,0:T(8,128)(2,1)} %copy-done.4) | copy-start | bytes 2162692
  388.8 10.5 %copy-start.9 = (bf16[512,2048]{1,0:T(8,128)(2,1)S(1)}, bf16[512,2048]{1,0:T(8,128)(2,1)}, u32[]{:S(2)}) copy-start(bf16[512,2048]{1,0:T(8,128)(2,1)} %all-gather.7.cloned.1.call-done) | copy-start | bytes 6291460
  399.3 15.8 %copy-start.8 = (bf16[2048]{0:T(1024)(128)(2,1)S(1)}, bf16[2048]{0:T(1024)(128)(2,1)}, u32[]{:S(2)}) copy-start(bf16[2048]{0:T(1024)(128)(2,1)} %param.23) | copy-start | bytes 12292
Sparse Core Ops, SparseCore 0:
  12.2 25.2 all-gather.4
  123.1 32.5 reduce-scatter.2
  415.2 30.0 reduce-scatter.4
Sparse Core Ops, SparseCore 1:
  125.7 118.8 all-gather.8
  246.0 33.3 all-gather.6
  281.4 117.8 all-gather.10
